TPU v7x, 32 devices: a whole 2x2x4 slice. The times are simulated.
32 devices in a mesh: ep: 4 (over y, x), tp: 8 (over z, core).
Axes of the slice: x: 2, y: 2, z: 4, core: 2. Of those that a mesh axis runs over, the one named last changes fastest.
Arguments:
- queries: bfloat16 [16, 64, 2, 512], P('tp', None, None, 'ep'), may hold values from -24 to 24
- key_vectors: bfloat16 [16, 64, 2, 512], P('tp', None, None, 'ep'), may hold values from -24 to 24
- value_vectors: bfloat16 [16, 64, 2, 512], P('tp', None, None, 'ep'), may hold values from -6 to 6
- mixer_weight: bfloat16 [1024, 2048], replicated, may hold values from -0.375 to 0.375
- expert_rows: bfloat16 [512, 2048], P('ep'), may hold values from -6 to 6
- norm_gain: float32 [2048], replicated, may hold values from 0.1 to 1.9
- route_ids: int32 [512, 2], P('ep'), may hold values from 0 to 7, all different within a row; in each aligned block of 128 rows (0 to 127, 128 to 255, ...) at most 64 rows name the same one
- route_logits: float32 [512, 2], P('ep'), may hold values from -4 to 4
- gate_weight: bfloat16 [8, 2048, 4096], P('ep', None, 'tp'), may hold values from -0.39648438 to 0.39648438
- up_weight: bfloat16 [8, 2048, 4096], P('ep', None, 'tp'), may hold values from -0.39648438 to 0.39648438
- down_weight: bfloat16 [8, 4096, 2048], P('ep', 'tp'), may hold values from -0.028076172 to 0.028076172
Outputs:
- mixer_out: bfloat16 [2, 512, 2048], P(None, ('ep', 'tp'))
- routed_out: bfloat16 [2048, 512], P('tp', 'ep')
Inputs may be any that keep to these rules, and one draw needn't show every extreme that they name: `route_ids`: each row names 2 different experts. Among the 128 rows of one index of ep no expert is named more than 64 times, a bound that some expert reaches in such a block.
All inputs are finite; a program needn't handle non-finite values.
Results may differ from a plain program's by a relative error of at most 0.018.
Values may be sent and summed in bfloat16 or wider, within the bound.
No kernel may reach another device: no remote copies, remote signals or barrier semaphores. Data moves between devices by JAX's collectives and lax.ppermute only.
A program may use at most 64 MiB of HBM per device.

v0:
```python
import jax
import jax.numpy as jnp
from jax import lax
from jax.sharding import PartitionSpec as P

limit_value = 7.0
alpha_value = 1.702
norm_eps = 1e-06


def activate(gate_pre, up_pre):
    gate_clamped = jnp.minimum(gate_pre, limit_value)
    up_clamped = jnp.clip(up_pre, -limit_value, limit_value)
    return ((up_clamped + 1.0) * gate_clamped * jax.nn.sigmoid(alpha_value * gate_clamped)).astype(
        jnp.bfloat16
    )


def block_terms(query_rows, key_block, value_block, block_index, own_index):
    seg_len = query_rows.shape[3]
    score_scale = query_rows.shape[1] ** (-0.5)
    scores = (
        jnp.einsum("hdsq,hdsk->hsqk", query_rows, key_block, preferred_element_type=jnp.float32)
        * score_scale
    )
    query_pos = lax.broadcasted_iota(jnp.int32, (seg_len, seg_len), 0)
    lookup_slot = lax.broadcasted_iota(jnp.int32, (seg_len, seg_len), 1)
    usable = jnp.logical_or(block_index < own_index, lookup_slot < query_pos)
    log_keep = jnp.where(usable, jax.nn.log_sigmoid(-scores), 0.0)
    within = lax.cumsum(log_keep, axis=3, reverse=True) - log_keep
    weight = jnp.where(usable, jnp.exp(jax.nn.log_sigmoid(scores) + within), 0.0).astype(
        jnp.bfloat16
    )
    block_out = jnp.einsum(
        "hsqk,hdsk->hdsq", weight, value_block, preferred_element_type=jnp.float32
    )
    return (block_out, jnp.sum(log_keep, axis=3))


def attend(query_rows, key_vectors, value_vectors):
    head_count, head_dim, seq_count, seg_len = query_rows.shape
    blocks = lax.axis_size("ep")
    own_index = lax.axis_index("ep")
    first_outs = jnp.zeros((blocks, head_count, head_dim, seq_count, seg_len), jnp.float32)
    first_totals = jnp.zeros((blocks, head_count, seq_count, seg_len), jnp.float32)
    key_piece = lax.all_gather(key_vectors, "ep", axis=3, tiled=True)
    value_piece = lax.all_gather(value_vectors, "ep", axis=3, tiled=True)
    shard_count = key_piece.shape[3] // seg_len

    def one_block(offset, inner_state):
        block_outs, block_totals = inner_state
        key_block = lax.dynamic_slice_in_dim(key_piece, offset * seg_len, seg_len, 3)
        value_block = lax.dynamic_slice_in_dim(value_piece, offset * seg_len, seg_len, 3)

        def compute(unused):
            return block_terms(query_rows, key_block, value_block, offset, own_index)

        def skip_block(unused):
            return (
                jnp.zeros((head_count, head_dim, seq_count, seg_len), jnp.float32),
                jnp.zeros((head_count, seq_count, seg_len), jnp.float32),
            )

        block_out, block_total = lax.cond(offset <= own_index, compute, skip_block, 0)
        block_outs = lax.dynamic_update_index_in_dim(block_outs, block_out, offset, 0)
        block_totals = lax.dynamic_update_index_in_dim(block_totals, block_total, offset, 0)
        return (block_outs, block_totals)

    block_outs, block_totals = lax.fori_loop(0, shard_count, one_block, (first_outs, first_totals))
    later_sums = lax.cumsum(block_totals, axis=0, reverse=True) - block_totals
    return jnp.sum(jnp.exp(later_sums)[:, :, None] * block_outs, axis=0).astype(jnp.bfloat16)


def mix_heads(attended, mixer_weight):
    head_count, head_dim, seq_count, seg_len = attended.shape
    flat_heads = attended.reshape(head_count * head_dim, seq_count, seg_len)
    return jnp.einsum(
        "csr,cm->srm",
        lax.all_to_all(flat_heads, "tp", split_axis=2, concat_axis=0, tiled=True),
        mixer_weight,
        preferred_element_type=jnp.float32,
    ).astype(jnp.bfloat16)


def expert_block(send_rows, gate_portion, up_part, down_part):
    groups = lax.axis_size("ep")
    local_experts = gate_portion.shape[0]
    cap_rows = send_rows.shape[1]
    model_width = send_rows.shape[2]
    received = lax.all_to_all(send_rows, "ep", split_axis=0, concat_axis=0, tiled=True)
    bucketed = received.reshape(groups, local_experts, cap_rows, model_width)
    gate_pre = jnp.einsum(
        "sjcd,jdf->sjcf", bucketed, gate_portion, preferred_element_type=jnp.float32
    )
    up_pre = jnp.einsum("sjcd,jdf->sjcf", bucketed, up_part, preferred_element_type=jnp.float32)
    hidden = activate(gate_pre, up_pre)
    slot_total = groups * local_experts * cap_rows
    term_rows = jnp.einsum("sjcf,jfd->dsjc", hidden, down_part, preferred_element_type=jnp.float32)
    summed = lax.psum_scatter(
        term_rows.reshape(
            model_width // lax.axis_size("tp") * lax.axis_size("tp"), slot_total
        ).astype(jnp.bfloat16),
        "tp",
        scatter_dimension=0,
        tiled=True,
    ).astype(jnp.float32)
    return lax.all_to_all(
        summed.astype(jnp.bfloat16), "ep", split_axis=1, concat_axis=1, tiled=True
    ).astype(summed.dtype)


def route_experts(
    expert_rows, norm_gain, route_ids, route_logits, gate_weight, up_weight, down_weight
):
    groups = lax.axis_size("ep")
    local_experts = gate_weight.shape[0]
    expert_count = groups * local_experts
    token_rows, top_count = route_ids.shape
    cap_rows = 2 * token_rows * top_count // expert_count
    values = expert_rows.astype(jnp.float32)
    scaled = values * lax.rsqrt(jnp.mean(values * values, axis=-1, keepdims=True) + norm_eps)
    normed = (scaled * norm_gain).astype(jnp.bfloat16)
    route_weight = jax.nn.softmax(route_logits, axis=-1)
    flat_ids = route_ids.reshape(token_rows * top_count)
    one_hot_matrix = (
        flat_ids[:, None] == jnp.arange(expert_count, dtype=jnp.int32)[None, :]
    ).astype(jnp.int32)
    earlier = jnp.cumsum(one_hot_matrix, axis=0) - one_hot_matrix
    slot_rank = jnp.sum(earlier * one_hot_matrix, axis=1)
    column = flat_ids * cap_rows + slot_rank
    token_index = jnp.arange(token_rows * top_count, dtype=jnp.int32) // top_count
    owner_token = jnp.zeros((expert_count * cap_rows,), jnp.int32).at[column].set(token_index)
    filled = jnp.zeros((expert_count * cap_rows,), jnp.int32).at[column].set(1)
    send_rows = jnp.where(filled[:, None] > 0, normed[owner_token], jnp.zeros((), jnp.bfloat16))
    send_rows = send_rows.reshape(groups, local_experts, cap_rows, normed.shape[1])
    halves = 1
    per_half = local_experts // halves
    part_rows = send_rows.reshape(groups * per_half, cap_rows, normed.shape[1])
    result = expert_block(part_rows, gate_weight, up_weight, down_weight)
    results = result.reshape(result.shape[0], groups, per_half, cap_rows)
    gathered = results.reshape(results.shape[0], expert_count * cap_rows)
    picked = jnp.take(gathered, column, axis=1).reshape(gathered.shape[0], token_rows, top_count)
    combined = jnp.sum(picked * route_weight[None], axis=2)
    return combined.astype(jnp.bfloat16)


def body(
    queries,
    key_vectors,
    value_vectors,
    mixer_weight,
    expert_rows,
    norm_gain,
    route_ids,
    route_logits,
    gate_weight,
    up_weight,
    down_weight,
):
    attended = attend(queries, key_vectors, value_vectors)
    mixer_out = mix_heads(attended, mixer_weight)
    routed_out = route_experts(
        expert_rows, norm_gain, route_ids, route_logits, gate_weight, up_weight, down_weight
    )
    return (mixer_out, routed_out)


def solution(mesh):
    in_specs = (
        P("tp", None, None, "ep"),
        P("tp", None, None, "ep"),
        P("tp", None, None, "ep"),
        P(),
        P("ep", None),
        P(),
        P("ep", None),
        P("ep", None),
        P("ep", None, "tp"),
        P("ep", None, "tp"),
        P("ep", "tp", None),
    )
    out_specs = (P(None, ("ep", "tp"), None), P("tp", "ep"))
    return jax.shard_map(body, mesh=mesh, in_specs=in_specs, out_specs=out_specs, check_vma=False)
```

profile of v0, /device:TPU:0, one launch (start us, length us, event | category | flops | bytes accessed | tf_op | source)
XLA Modules:
  0.0 130.4 jit_solution(11275441368211532716)
XLA Ops:
  7.2 0.0 reduce-scatter.2.cloned.1.call-start
  7.2 0.8 copy.67
  8.0 0.1 eq.26
  8.1 0.1 reshape.99
  8.3 0.7 broadcast_multiply_fusion
  9.0 0.6 reduce-window.6
  9.6 0.2 slice_reduce_fusion
  9.8 0.1 copy.71
  9.9 0.1 mul.98
  10.1 0.1 fusion.87
  10.2 1.4 %scatter_custom_fusion.1 = s32[512]{0:T(512)S(1)} fusion(s32[256]{0:T(256)S(1)} %bitcast.93, s32[256]{0:T(256)S(1)} %and_select_fusion, s32[]{:T(128)} %copy.121), kind=kCustom, calls=%fused_computation.82 | custom fusion | bytes 2052 | tf_op jit(solution)/shard_map/scatter | solution.py:132
  11.6 1.2 fusion.73
  12.8 1.4 %scatter_custom_fusion = s32[512]{0:T(512)S(1)} fusion(s32[256]{0:T(256)S(1)} %bitcast.94, s32[256]{0:T(256)S(1)} %broadcast.130, s32[]{:T(128)} %copy.121), kind=kCustom, calls=%fused_computation.85 | custom fusion | bytes 2052 | tf_op jit(solution)/shard_map/scatter | solution.py:133
  14.3 0.1 broadcast_in_dim.94
  14.3 1.2 fusion.75
  15.6 2.5 %gather_fusion = bf16[512,2048]{1,0:T(8,128)(2,1)S(1)} fusion(bf16[128,2048]{1,0:T(8,128)(2,1)S(1)} %fusion.75, s32[1024]{0:T(1024)S(1)} %pad_clamp_fusion.1), kind=kCustom, calls=%fused_computation | custom fusion | bytes 4196352 | tf_op jit(solution)/shard_map/gather | solution.py:134
  18.1 0.2 broadcast_select_fusion
  18.3 0.0 copy-start.5
  18.3 30.6 %all_to_all.32 = bf16[8,64,2048]{2,1,0:T(8,128)(2,1)S(1)} all-to-all(bf16[8,64,2048]{2,1,0:T(8,128)(2,1)S(1)} %broadcast_select_fusion), channel_id=1, replica_groups=mesh['ep'=4,'tp'=8] {'ep'}, dimensions={0} | all-to-all | bytes 4194304 | tf_op jit(solution)/shard_map/all_to_all | solution.py:90
  48.9 0.0 copy-done.5
  48.9 1.2 fusion.57
  50.2 7.3 %fusion.29 = bf16[2048,4,2,64]{0,3,1,2:T(8,128)(2,1)} fusion(bf16[2,512,2048]{2,1,0:T(8,128)(2,1)} %param.25, f32[2,4,64,512]{3,2,1,0:T(8,128)S(1)} %fusion.57, bf16[2,2048,512]{2,1,0:T(8,128)(2,1)} %param.24, bf16[4,2,64,2048]{3,2,1,0:T(8,128)(2,1)S(1)} %bitcast.86), kind=kOutput, calls=%fused_computation.36 | convolution fusion | flops 2150891520 | bytes 13631488 | tf_op jit(solution)/shard_map/sjcf,jfd->dsjc/dot_general | solution.py:98
  57.4 3.2 %copy.74 = bf16[2048,4,2,64]{0,3,2,1:T(8,128)(2,1)} copy(bf16[2048,4,2,64]{0,3,1,2:T(8,128)(2,1)} %fusion.29) | data formatting | bytes 4194304 | tf_op jit(solution)/shard_map/convert_element_type | solution.py:102
  60.6 0.0 copy-start
  60.6 0.0 copy-start.1
  60.6 0.0 copy-start.2
  60.6 0.0 reduce-scatter.2.cloned.1.call-update
  60.7 0.8 copy-done
  61.5 0.0 copy-done.1
  61.5 0.0 copy-done.2
  61.6 8.6 %all_gather.6 = bf16[2,64,2,512]{3,1,2,0:T(8,128)(2,1)S(1)} all-gather(bf16[2,64,2,128]{3,1,2,0:T(8,128)(2,1)S(1)} %copy.60), channel_id=1, replica_groups=mesh['ep'=4,'tp'=8] {'ep'}, dimensions={3}, use_global_device_ids=true | all-gather | bytes 327680 | tf_op jit(solution)/shard_map/all_gather | solution.py:46
  70.2 8.9 %all_gather.7 = bf16[2,64,2,512]{3,1,2,0:T(8,128)(2,1)S(1)} all-gather(bf16[2,64,2,128]{3,1,2,0:T(8,128)(2,1)S(1)} %copy.61), channel_id=1, replica_groups=mesh['ep'=4,'tp'=8] {'ep'}, dimensions={3}, use_global_device_ids=true | all-gather | bytes 327680 | tf_op jit(solution)/shard_map/all_gather | solution.py:47
  79.0 0.0 copy-start.4
  79.1 0.0 copy-start.3
  79.1 5.8 %while.15 = (s32[]{:T(128)}, f32[4,2,64,2,128]{4,2,3,1,0:T(8,128)S(1)}, f32[4,2,2,128]{3,2,1,0:T(2,128)S(1)}, s32[]{:T(128)}, bf16[2,64,2,512]{3,1,2,0:T(8,128)(...) while((s32[]{:T(128)}, ...), condition=%wide.region_5.6_spmd, body=%wide.region_0.5_spmd.sunk | while | flops 27098632 | bytes 2218215 | solution.py:69
  79.1 5.4 %conditional.2 = (f32[1,2,64,2,128]{4,2,3,1,0:T(8,128)S(1)}, f32[1,2,2,128]{3,2,1,0:T(2,128)S(1)}) conditional(s32[]{:T(128)} %convert_element_type.99, () %tuple.66, (s32[]{:T(128)}, s32[]{:T(128)}, bf16[2,64,2,512]{3,1,2,0:T(8,128)(2,1)S(1)}, bf16[2,64,2,128]{3,1,2,0:T(8,128)(2,1)S(1)}, bf16[2,64,2,512]{3,1,2,0:T(8,128)(2,1)S(1)}) %tuple.67), branch_computations={%region_1.0_spmd, %region_2.4_spmd} | conditional | flops 27098628 | bytes 1951828 | solution.py:64
  79.1 0.4 fusion.16
  79.5 4.4 %reduce_window_sum.35 = f32[2,2,128,128]{2,3,1,0:T(8,128)S(1)} reduce-window(f32[2,2,128,128]{2,3,1,0:T(8,128)S(1)} %get-tuple-element.277, f32[]{:T(128)} %constant.130.clone), window={size=1x1x1x128 pad=0_0x0_0x0_0x0_127}, to_apply=%region_3.2 | reduce-window | flops 8323072 | bytes 524292 | tf_op jit(solution)/shard_map/while/body/eval_jaxpr/cond/branch_1_fun/reduce_window_sum | solution.py:30
  84.0 0.5 convolution_bitcast_fusion
  84.9 0.8 copy.64
  85.7 4.9 %all-to-all-start = ((bf16[128,2,128]{0,1,2:T(2,128)(2,1)}), bf16[128,2,128]{0,1,2:T(2,128)(2,1)S(1)}, u32[]{:S(2)}, u32[]{:S(2)}) async-start(bf16[128,2,128]{0,1,2:T(2,128)(2,1)} %copy.64), calls=%async_computation | async-start | bytes 131072 | tf_op jit(solution)/shard_map/all_to_all | solution.py:79
  90.6 0.1 reduce_sum.64
  90.7 0.1 copy.69
  90.8 0.0 copy-done.4
  90.9 0.0 copy-done.3
  90.9 0.1 copy.70
  91.0 0.1 copy.75
  91.1 5.4 %all-to-all-done = bf16[128,2,128]{0,1,2:T(2,128)(2,1)S(1)} async-done(((bf16[128,2,128]{0,1,2:T(2,128)(2,1)}), bf16[128,2,128]{0,1,2:T(2,128)(2,1)S(1)}, u32[]{:S(2)}, u32[]{:S(2)}) %all-to-all-start) | async-done | bytes 65568 | tf_op jit(solution)/shard_map/all_to_all | solution.py:79
  96.5 0.3 reduce-scatter.2.cloned.1.call-done
  96.8 18.6 %all-to-all-start.2 = ((bf16[256,4,128]{0,2,1:T(8,128)(2,1)}), bf16[256,4,128]{0,2,1:T(8,128)(2,1)S(1)}, u32[]{:S(2)}, u32[]{:S(2)}) async-start(bf16[256,4,128]{0,2,1:T(8,128)(2,1)} %bitcast.89), calls=%async_computation.3 | async-start | bytes 524288 | tf_op jit(solution)/shard_map/all_to_all | solution.py:107
  115.3 3.7 %fusion.32 = bf16[2,16,2048]{2,1,0:T(8,128)(2,1)} fusion(bf16[1024,2048]{1,0:T(8,128)(2,1)} %param.18, bf16[2,8,2,8,128]{4,3,2,1,0:T(8,128)(2,1)S(1)} %bitcast.88), kind=kOutput, calls=%fused_computation.37 | convolution fusion | flops 134283264 | bytes 4390912 | tf_op jit(solution)/shard_map/csr,cm->srm/dot_general | solution.py:77
  119.0 1.7 %all-to-all-done.2 = bf16[256,4,128]{0,2,1:T(8,128)(2,1)S(1)} async-done(((bf16[256,4,128]{0,2,1:T(8,128)(2,1)}), bf16[256,4,128]{0,2,1:T(8,128)(2,1)S(1)}, u32[]{:S(2)}, u32[]{:S(2)}) %all-to-all-start.2) | async-done | bytes 262176 | tf_op jit(solution)/shard_map/all_to_all | solution.py:107
  120.7 0.1 bitcast_convert_fusion
  120.8 1.0 gather_fusion.1
  121.7 0.1 gather.14
  121.9 0.9 multiply_reduce_fusion.1
  122.8 0.7 copy.76
  (42 shorter events, 0.6 us)
Async XLA Ops:
  7.2 89.6 %reduce-scatter.2.cloned.1.call-start = ((), (), s32[]{:S(2)}) async-start(), calls=%async_computation.4 | async-start | bytes 2359296 | tf_op jit(solution)/shard_map/reduce_scatter | solution.py:99
  18.3 30.6 %copy-start.5 = (bf16[2,2048,512]{2,1,0:T(8,128)(2,1)S(1)}, bf16[2,2048,512]{2,1,0:T(8,128)(2,1)}, u32[]{:S(2)}) copy-start(bf16[2,2048,512]{2,1,0:T(8,128)(2,1)} %param.23) | copy-start | bytes 12582916
  60.6 0.8 copy-start
  60.6 0.9 copy-start.1
  60.6 0.9 copy-start.2
  79.0 11.7 %copy-start.4 = (f32[128,2]{0,1:T(2,128)S(1)}, f32[128,2]{0,1:T(2,128)}, u32[]{:S(2)}) copy-start(f32[128,2]{0,1:T(2,128)} %param.22) | copy-start | bytes 3076
  79.1 11.8 %copy-start.3 = (s32[128,2]{0,1:T(2,128)S(1)}, s32[128,2]{0,1:T(2,128)}, u32[]{:S(2)}) copy-start(s32[128,2]{0,1:T(2,128)} %param.21) | copy-start | bytes 3076
  85.7 10.8 %all-to-all-start = ((bf16[128,2,128]{0,1,2:T(2,128)(2,1)}), bf16[128,2,128]{0,1,2:T(2,128)(2,1)S(1)}, u32[]{:S(2)}, u32[]{:S(2)}) async-start(bf16[128,2,128]{0,1,2:T(2,128)(2,1)} %copy.64), calls=%async_computation | async-start | bytes 131072 | tf_op jit(solution)/shard_map/all_to_all | solution.py:79
  96.8 23.9 %all-to-all-start.2 = ((bf16[256,4,128]{0,2,1:T(8,128)(2,1)}), bf16[256,4,128]{0,2,1:T(8,128)(2,1)S(1)}, u32[]{:S(2)}, u32[]{:S(2)}) async-start(bf16[256,4,128]{0,2,1:T(8,128)(2,1)} %bitcast.89), calls=%async_computation.3 | async-start | bytes 524288 | tf_op jit(solution)/shard_map/all_to_all | solution.py:107
Sparse Core Ops, SparseCore 0:
  60.8 35.9 reduce-scatter.1
where the time goes:
time: 131 us; the launch traced here: 130 us
  blocking collectives  48.1 us (37%)
  starting transfers between devices  23.5 us (18%)
  between operations  14.3 us (11%)
  local copies, waits for them, and re-layouts  14.2 us (11%)
  matrix products  13.1 us (10%)
  other arithmetic  9.63 us (7%)
  waiting for transfers between devices  7.31 us (6%)
    all_to_all x1, blocking collectives, expert_block(): lax.all_to_all(send_rows, 'ep', split_axis=0, concat_axis=0, tiled=True)  30.6 us
    all_to_all x1, starting transfers between devices, expert_block(): lax.all_to_all(summed.astype(jnp.bfloat16), 'ep', split_axis=1, concat_ax...  18.6 us
    all_gather x1, blocking collectives, attend(): value_piece = lax.all_gather(value_vectors, 'ep', axis=3, tiled=True)  8.89 us
    all_gather x1, blocking collectives, attend(): key_piece = lax.all_gather(key_vectors, 'ep', axis=3, tiled=True)  8.6 us
    dot_general x1, matrix products, expert_block(): jnp.einsum('sjcf,jfd->dsjc', hidden, down_part, preferred_element_type=jn...  7.28 us
    all_to_all x1, waiting for transfers between devices, mix_heads(): lax.all_to_all(flat_heads, 'tp', split_axis=2, concat_axis=0, tiled=True)  5.35 us
    all_to_all x1, starting transfers between devices, mix_heads(): lax.all_to_all(flat_heads, 'tp', split_axis=2, concat_axis=0, tiled=True)  4.88 us
    another operation x1, other arithmetic, block_terms(): within = lax.cumsum(log_keep, axis=3, reverse=True) - log_keep  4.43 us
  transfers between devices with their start and end apart: 3, of which 3 were waited for; matrix products, arithmetic and copies ran while one was open for 8% of the time, Pallas kernels for 0%

commit v1 on v0

--- a/solution.py
+++ b/solution.py
@@ -76,7 +76,12 @@
     flat_heads = attended.reshape(head_count * head_dim, seq_count, seg_len)
     return jnp.einsum(
         "csr,cm->srm",
-        lax.all_to_all(flat_heads, "tp", split_axis=2, concat_axis=0, tiled=True),
+        jnp.concatenate(
+            lax.all_to_all(
+                jnp.stack(jnp.split(flat_heads, lax.axis_size("tp"), axis=2)), "tp", 0, 0
+            ),
+            axis=0,
+        ),
         mixer_weight,
         preferred_element_type=jnp.float32,
     ).astype(jnp.bfloat16)

time: 131 us -> 136 us (1.038)
  local copies, waits for them, and re-layouts: 14.2 us -> 19.1 us
    unnamed x16 -> x23, local copies, waits for them, and re-layouts: 2.38 us -> 6.61 us
  transfers between devices with their start and end apart: 3 -> 3, of which waited for: 3 -> 2; matrix products, arithmetic and copies ran while one was open for 8% -> 11% of each run, Pallas kernels for 0% -> 0%
where the time goes in v1:
time: 136 us; the launch traced here: 135 us
  blocking collectives  48.1 us (35%)
  starting transfers between devices  23.7 us (17%)
  local copies, waits for them, and re-layouts  19.1 us (14%)
  between operations  14.3 us (11%)
  matrix products  13.2 us (10%)
  other arithmetic  9.63 us (7%)
  waiting for transfers between devices  7.06 us (5%)
    all_to_all x1, blocking collectives, expert_block(): lax.all_to_all(send_rows, 'ep', split_axis=0, concat_axis=0, tiled=True)  30.6 us
    all_to_all x1, starting transfers between devices, expert_block(): lax.all_to_all(summed.astype(jnp.bfloat16), 'ep', split_axis=1, concat_ax...  18.8 us
    all_gather x1, blocking collectives, attend(): value_piece = lax.all_gather(value_vectors, 'ep', axis=3, tiled=True)  8.9 us
    all_gather x1, blocking collectives, attend(): key_piece = lax.all_gather(key_vectors, 'ep', axis=3, tiled=True)  8.59 us
    dot_general x1, matrix products, expert_block(): jnp.einsum('sjcf,jfd->dsjc', hidden, down_part, preferred_element_type=jn...  7.28 us
    unnamed x23, local copies, waits for them, and re-layouts  6.61 us
    all_to_all x1, waiting for transfers between devices, mix_heads(): lax.all_to_all(jnp.stack(jnp.split(flat_heads, lax.axis_size('tp'), axis=...  5.35 us
    all_to_all x1, starting transfers between devices, mix_heads(): lax.all_to_all(jnp.stack(jnp.split(flat_heads, lax.axis_size('tp'), axis=...  4.87 us
  transfers between devices with their start and end apart: 3, of which 2 were waited for; matrix products, arithmetic and copies ran while one was open for 11% of the time, Pallas kernels for 0%

profile of v1, /device:TPU:0, one launch (start us, length us, event | category | flops | bytes accessed | tf_op | source)
XLA Modules:
  0.0 135.3 jit_solution(4806089767754870516)
XLA Ops:
  7.2 0.0 reduce-scatter.2.cloned.1.call-start
  7.2 0.8 copy.75
  8.0 0.1 eq.26
  8.1 0.1 reshape.103
  8.3 0.7 broadcast_multiply_fusion
  9.0 0.6 reduce-window.6
  9.6 0.2 slice_reduce_fusion
  9.8 0.1 copy.79
  9.9 0.1 mul.98
  10.1 0.1 fusion.87
  10.2 1.4 %scatter_custom_fusion.1 = s32[512]{0:T(512)S(1)} fusion(s32[256]{0:T(256)S(1)} %bitcast.108, s32[256]{0:T(256)S(1)} %and_select_fusion, s32[]{:T(128)} %copy.136), kind=kCustom, calls=%fused_computation.97 | custom fusion | bytes 2052 | tf_op jit(solution)/shard_map/scatter | solution.py:137
  11.6 1.2 fusion.73
  12.8 1.4 %scatter_custom_fusion = s32[512]{0:T(512)S(1)} fusion(s32[256]{0:T(256)S(1)} %bitcast.109, s32[256]{0:T(256)S(1)} %broadcast.130, s32[]{:T(128)} %copy.136), kind=kCustom, calls=%fused_computation.100 | custom fusion | bytes 2052 | tf_op jit(solution)/shard_map/scatter | solution.py:138
  14.3 0.1 broadcast_in_dim.94
  14.3 1.2 fusion.75
  15.6 2.5 %gather_fusion = bf16[512,2048]{1,0:T(8,128)(2,1)S(1)} fusion(bf16[128,2048]{1,0:T(8,128)(2,1)S(1)} %fusion.75, s32[1024]{0:T(1024)S(1)} %pad_clamp_fusion.1), kind=kCustom, calls=%fused_computation | custom fusion | bytes 4196352 | tf_op jit(solution)/shard_map/gather | solution.py:139
  18.1 0.2 broadcast_select_fusion
  18.3 0.0 copy-start.5
  18.3 30.6 %all_to_all.19 = bf16[8,64,2048]{2,1,0:T(8,128)(2,1)S(1)} all-to-all(bf16[8,64,2048]{2,1,0:T(8,128)(2,1)S(1)} %broadcast_select_fusion), channel_id=1, replica_groups=mesh['ep'=4,'tp'=8] {'ep'}, dimensions={0} | all-to-all | bytes 4194304 | tf_op jit(solution)/shard_map/all_to_all | solution.py:95
  48.9 1.3 fusion.57
  50.2 7.3 %fusion.29 = bf16[2048,4,2,64]{0,3,1,2:T(8,128)(2,1)} fusion(bf16[2,512,2048]{2,1,0:T(8,128)(2,1)} %param.25, f32[2,4,64,512]{3,2,1,0:T(8,128)S(1)} %fusion.57, bf16[2,2048,512]{2,1,0:T(8,128)(2,1)} %param.24, bf16[4,2,64,2048]{3,2,1,0:T(8,128)(2,1)S(1)} %bitcast.103), kind=kOutput, calls=%fused_computation.36 | convolution fusion | flops 2150891520 | bytes 13631488 | tf_op jit(solution)/shard_map/sjcf,jfd->dsjc/dot_general | solution.py:103
  57.5 3.2 %copy.82 = bf16[2048,4,2,64]{0,3,2,1:T(8,128)(2,1)} copy(bf16[2048,4,2,64]{0,3,1,2:T(8,128)(2,1)} %fusion.29) | data formatting | bytes 4194304 | tf_op jit(solution)/shard_map/convert_element_type | solution.py:107
  60.7 0.0 reduce-scatter.2.cloned.1.call-update
  60.7 0.8 copy-done
  61.5 0.0 copy-done.1
  61.6 0.0 copy-done.2
  61.6 8.6 %all_gather.6 = bf16[2,64,2,512]{3,1,2,0:T(8,128)(2,1)S(1)} all-gather(bf16[2,64,2,128]{3,1,2,0:T(8,128)(2,1)S(1)} %copy.62), channel_id=1, replica_groups=mesh['ep'=4,'tp'=8] {'ep'}, dimensions={3}, use_global_device_ids=true | all-gather | bytes 327680 | tf_op jit(solution)/shard_map/all_gather | solution.py:46
  70.2 8.9 %all_gather.7 = bf16[2,64,2,512]{3,1,2,0:T(8,128)(2,1)S(1)} all-gather(bf16[2,64,2,128]{3,1,2,0:T(8,128)(2,1)S(1)} %copy.63), channel_id=1, replica_groups=mesh['ep'=4,'tp'=8] {'ep'}, dimensions={3}, use_global_device_ids=true | all-gather | bytes 327680 | tf_op jit(solution)/shard_map/all_gather | solution.py:47
  79.1 5.7 %while.15 = (s32[]{:T(128)}, f32[4,2,64,2,128]{4,2,3,1,0:T(8,128)S(1)}, f32[4,2,2,128]{3,2,1,0:T(2,128)S(1)}, s32[]{:T(128)}, bf16[2,64,2,512]{3,1,2,0:T(8,128)(...) while((s32[]{:T(128)}, ...), condition=%wide.region_5.6_spmd, body=%wide.region_0.5_spmd.sunk | while | flops 27098632 | bytes 2218215 | solution.py:69
  79.1 5.4 %conditional.2 = (f32[1,2,64,2,128]{4,2,3,1,0:T(8,128)S(1)}, f32[1,2,2,128]{3,2,1,0:T(2,128)S(1)}) conditional(s32[]{:T(128)} %convert_element_type.99, () %tuple.72, (s32[]{:T(128)}, s32[]{:T(128)}, bf16[2,64,2,512]{3,1,2,0:T(8,128)(2,1)S(1)}, bf16[2,64,2,128]{3,1,2,0:T(8,128)(2,1)S(1)}, bf16[2,64,2,512]{3,1,2,0:T(8,128)(2,1)S(1)}) %tuple.73), branch_computations={%region_1.0_spmd, %region_2.4_spmd} | conditional | flops 27098628 | bytes 1951828 | solution.py:64
  79.1 0.4 fusion.16
  79.5 4.4 %reduce_window_sum.35 = f32[2,2,128,128]{2,3,1,0:T(8,128)S(1)} reduce-window(f32[2,2,128,128]{2,3,1,0:T(8,128)S(1)} %get-tuple-element.270, f32[]{:T(128)} %constant.130.clone), window={size=1x1x1x128 pad=0_0x0_0x0_0x0_127}, to_apply=%region_3.2 | reduce-window | flops 8323072 | bytes 524292 | tf_op jit(solution)/shard_map/while/body/eval_jaxpr/cond/branch_1_fun/reduce_window_sum | solution.py:30
  84.0 0.5 convolution_bitcast_fusion
  85.0 0.2 fusion.99
  85.2 0.1 copy.67
  85.2 0.1 copy.68
  85.3 0.1 copy.69
  85.4 0.1 copy.70
  85.5 0.1 copy.71
  85.6 0.1 copy.72
  85.7 0.1 copy.73
  85.8 0.1 copy.66
  85.8 0.6 constant_dynamic-update-slice_fusion.9
  86.5 0.6 constant_dynamic-update-slice_fusion.8
  87.1 0.6 constant_dynamic-update-slice_fusion.7
  87.7 0.6 constant_dynamic-update-slice_fusion.6
  88.3 0.6 constant_dynamic-update-slice_fusion.5
  88.9 0.6 constant_dynamic-update-slice_fusion.4
  89.5 0.6 constant_dynamic-update-slice_fusion.3
  90.1 0.6 constant_dynamic-update-slice_fusion.2
  90.7 4.9 %all-to-all-start = ((bf16[8,128,2,16]{1,3,2,0:T(8,128)(2,1)}), bf16[8,128,2,16]{1,3,2,0:T(8,128)(2,1)S(1)}, u32[]{:S(2)}, u32[]{:S(2)}) async-start(bf16[8,128,2,16]{1,3,2,0:T(8,128)(2,1)} %constant_dynamic-update-slice_fusion.2), calls=%async_computation | async-start | bytes 131072 | tf_op jit(solution)/shard_map/all_to_all | solution.py:80
  95.5 0.1 reduce_sum.64
  95.7 0.1 copy.77
  95.8 0.1 copy.78
  96.0 0.1 copy.83
  96.1 5.4 %all-to-all-done = bf16[8,128,2,16]{1,3,2,0:T(8,128)(2,1)S(1)} async-done(((bf16[8,128,2,16]{1,3,2,0:T(8,128)(2,1)}), bf16[8,128,2,16]{1,3,2,0:T(8,128)(2,1)S(1)}, u32[]{:S(2)}, u32[]{:S(2)}) %all-to-all-start) | async-done | bytes 65568 | tf_op jit(solution)/shard_map/all_to_all | solution.py:80
  101.5 18.8 %all-to-all-start.2 = ((bf16[256,4,128]{0,2,1:T(8,128)(2,1)}), bf16[256,4,128]{0,2,1:T(8,128)(2,1)S(1)}, u32[]{:S(2)}, u32[]{:S(2)}) async-start(bf16[256,4,128]{0,2,1:T(8,128)(2,1)} %bitcast.105), calls=%async_computation.3 | async-start | bytes 524288 | tf_op jit(solution)/shard_map/all_to_all | solution.py:112
  120.2 3.7 %fusion.32 = bf16[2,16,2048]{2,1,0:T(8,128)(2,1)} fusion(bf16[1024,2048]{1,0:T(8,128)(2,1)} %param.18, bf16[8,128,2,16]{1,3,2,0:T(8,128)(2,1)S(1)} %all-to-all-done), kind=kOutput, calls=%fused_computation.37 | convolution fusion | flops 134283264 | bytes 4390912 | tf_op jit(solution)/shard_map/csr,cm->srm/dot_general | solution.py:77
  123.9 1.7 %all-to-all-done.2 = bf16[256,4,128]{0,2,1:T(8,128)(2,1)S(1)} async-done(((bf16[256,4,128]{0,2,1:T(8,128)(2,1)}), bf16[256,4,128]{0,2,1:T(8,128)(2,1)S(1)}, u32[]{:S(2)}, u32[]{:S(2)}) %all-to-all-start.2) | async-done | bytes 262176 | tf_op jit(solution)/shard_map/all_to_all | solution.py:112
  125.6 0.1 bitcast_convert_fusion
  125.7 1.0 gather_fusion.1
  126.6 0.1 gather.14
  126.8 0.9 multiply_reduce_fusion.1
  127.7 0.7 copy.84
  (50 shorter events, 0.6 us)
Async XLA Ops:
  7.2 94.3 %reduce-scatter.2.cloned.1.call-start = ((), (), s32[]{:S(2)}) async-start(), calls=%async_computation.4 | async-start | bytes 2359296 | tf_op jit(solution)/shard_map/reduce_scatter | solution.py:104
  18.3 30.6 %copy-start.5 = (bf16[2,2048,512]{2,1,0:T(8,128)(2,1)S(1)}, bf16[2,2048,512]{2,1,0:T(8,128)(2,1)}, u32[]{:S(2)}) copy-start(bf16[2,2048,512]{2,1,0:T(8,128)(2,1)} %param.23) | copy-start | bytes 12582916
  60.7 0.8 copy-start
  60.7 0.9 copy-start.1
  60.7 0.9 copy-start.2
  84.8 10.9 %copy-start.4 = (f32[128,2]{0,1:T(2,128)S(1)}, f32[128,2]{0,1:T(2,128)}, u32[]{:S(2)}) copy-start(f32[128,2]{0,1:T(2,128)} %param.22) | copy-start | bytes 3076
  84.9 11.0 %copy-start.3 = (s32[128,2]{0,1:T(2,128)S(1)}, s32[128,2]{0,1:T(2,128)}, u32[]{:S(2)}) copy-start(s32[128,2]{0,1:T(2,128)} %param.21) | copy-start | bytes 3076
  90.7 10.8 %all-to-all-start = ((bf16[8,128,2,16]{1,3,2,0:T(8,128)(2,1)}), bf16[8,128,2,16]{1,3,2,0:T(8,128)(2,1)S(1)}, u32[]{:S(2)}, u32[]{:S(2)}) async-start(bf16[8,128,2,16]{1,3,2,0:T(8,128)(2,1)} %constant_dynamic-update-slice_fusion.2), calls=%async_computation | async-start | bytes 131072 | tf_op jit(solution)/shard_map/all_to_all | solution.py:80
  101.5 24.1 %all-to-all-start.2 = ((bf16[256,4,128]{0,2,1:T(8,128)(2,1)}), bf16[256,4,128]{0,2,1:T(8,128)(2,1)S(1)}, u32[]{:S(2)}, u32[]{:S(2)}) async-start(bf16[256,4,128]{0,2,1:T(8,128)(2,1)} %bitcast.105), calls=%async_computation.3 | async-start | bytes 524288 | tf_op jit(solution)/shard_map/all_to_all | solution.py:112
Sparse Core Ops, SparseCore 0:
  60.8 35.5 reduce-scatter.1
